TPU v7x, 32 devices: a whole 2x2x4 slice. The times are simulated.
32 devices in a mesh: grp: 2 (over y), sp: 4 (over z), tp: 4 (over x, core).
Axes of the slice: x: 2, y: 2, z: 4, core: 2. Of those that a mesh axis runs over, the one named last changes fastest.
Arguments:
- carryover_vector: bfloat16 [2048, 2048], P(('grp', 'sp', 'tp')), parts along dimension 0, may hold values from -6 to 6
- channel_source_entries: bfloat16 [2048, 1024], P(('grp', 'sp'), 'tp'), parts along dimension 0, may hold values from -6 to 6
- final_modulation_vector: bfloat16 [2048, 1024], P(('grp', 'sp'), 'tp'), parts along dimension 0, may hold values from -54 to 54
- entering_basis_matrix: bfloat16 [2048, 512], P(('grp', 'sp'), 'tp'), parts along dimension 0, may hold values from -6 to 6
- readout_basis_matrix: bfloat16 [2048, 512], P(('grp', 'sp'), 'tp'), parts along dimension 0, may hold values from -6 to 6
- raw_stride_amount: float32 [2048, 16], P(('grp', 'sp'), 'tp'), parts along dimension 0, may hold values from -6 to 5
- extra_log_attenuation: float32 [2048, 16], P(('grp', 'sp'), 'tp'), parts along dimension 0, may hold values from -1.4 to 0
- channel_fading_rate: float32 [16], P('tp'), may hold values from 0 to 0.1, as said below
- channel_source_kernel: float32 [4, 1024], P(None, 'tp'), may hold values from -3 to 3
- entering_basis_kernel: float32 [4, 512], P(None, 'tp'), may hold values from -3 to 3
- readout_basis_kernel: float32 [4, 512], P(None, 'tp'), may hold values from -3 to 3
- modulated_rescaling_vector: float32 [1024], replicated, may hold values from 0.1 to 1.9
- blender_final_matrix: bfloat16 [1024, 2048], replicated, may hold values from -0.1875 to 0.1875
- specialist_rescaling_vector: float32 [2048], replicated, may hold values from 0.1 to 1.9
- specialist_gating_matrices: bfloat16 [8, 2048, 1024], P('sp', None, 'tp'), may hold values from -0.125 to 0.125
- widening_matrices: bfloat16 [8, 2048, 1024], P('sp', None, 'tp'), may hold values from -0.125 to 0.125
- contracting_matrices: bfloat16 [8, 1024, 2048], P('sp', 'tp'), may hold values from -0.1875 to 0.1875
- assigned_specialist_ids: int32 [2048, 2], P(('grp', 'sp')), parts along dimension 0, may hold values from 0 to 7, as said below
- specialist_choice_affinity: float32 [2048, 2], P(('grp', 'sp', 'tp')), parts along dimension 0, may hold values from -6 to 6
- cluster_chance: float32 [2048], P(('grp', 'sp', 'tp')), parts along dimension 0, may hold values from 0.25 to 1
Outputs:
- layer_out: bfloat16 [2048, 2048], P(('grp', 'sp', 'tp')), parts along dimension 0
There are 2 independent parts, one for each index of `grp`. A program takes and returns all parts, laid end to end along the dimension named above; an argument that names none is the same for every part. Nothing has to cross between parts.
Inputs may be any that keep to these rules, and one draw needn't show every extreme that they name: `assigned_specialist_ids`: each row names 2 different experts of one group: the experts g * 2 to (g + 1) * 2 - 1 for one g below 4. In each aligned block of 64 rows (the rows of one device) no expert is named by more than 32 rows, and every expert of one group, the same group in all blocks, is named by exactly 32 rows of every block. `channel_fading_rate`: positive.
All inputs are finite; a program needn't handle non-finite values.
Results may differ from a plain program's by a relative error of at most 0.015.
Values may be sent and summed in bfloat16 or wider, within the bound.
A program may use at most 64 MiB of HBM per device.

v0:
```python
import jax
import jax.numpy as jnp
from jax import lax
from jax.sharding import PartitionSpec as P

HEAD_DIM = 64
STATE = 128
BLOCK = 64
EPS = 1e-06
HIGHEST = lax.Precision.HIGHEST


def prefix(x, axis, combine, identity):
    size, index = (lax.axis_size(axis), lax.axis_index(axis))
    everything = jax.tree.map(
        lambda part, kind: lax.all_gather(part.astype(kind), axis), x, (jnp.bfloat16, jnp.bfloat16)
    )
    start = jax.tree.map(
        lambda part, zero: jnp.broadcast_to(jnp.asarray(zero, part.dtype), part.shape), x, identity
    )

    def lap(k, before):
        reached = k < index
        new = combine(
            before, jax.tree.map(lambda part, own: part[k].astype(own.dtype), everything, x)
        )
        return jax.tree.map(lambda a, b: jnp.where(reached, a, b), new, before)

    return lax.fori_loop(0, size, lap, start)


def from_behind(x, axis, by):
    size = lax.axis_size(axis)
    pairs = [(i, i + by) for i in range(size) if 0 <= i + by < size]
    return lax.ppermute(x, axis, pairs)


def causal_conv(signal, earlier, weights):
    kernel_len = weights.shape[0]
    length = signal.shape[0]
    joined = jnp.concatenate([earlier, signal], axis=0).astype(jnp.float32)
    accumulated = jnp.zeros((length, signal.shape[1]), jnp.float32)
    for offset in range(kernel_len):
        accumulated = accumulated + weights[offset][None, :] * joined[offset : offset + length]
    return jax.nn.silu(accumulated)


def link_states(earlier, later):
    return (earlier[0] * later[0], earlier[1] * later[0][..., None, None] + later[1])


def device_states(scaled_in, log_attenuation, keys_b, queries_c, groups_here):
    length = scaled_in.shape[0]
    blocks = length // BLOCK
    per_group = scaled_in.shape[1] // groups_here
    scaled_in = scaled_in.reshape(blocks, BLOCK, groups_here, per_group, HEAD_DIM)
    log_attenuation = log_attenuation.reshape(blocks, BLOCK, groups_here, per_group)
    keys_b = keys_b.reshape(blocks, BLOCK, groups_here, STATE)
    queries_c = queries_c.reshape(blocks, BLOCK, groups_here, STATE)
    running = jnp.cumsum(log_attenuation, axis=1)
    lower_mask = jnp.tril(jnp.ones((BLOCK, BLOCK), dtype=bool))
    between = running[:, :, None] - running[:, None, :]
    decays = jnp.exp(jnp.where(lower_mask[None, :, :, None, None], between, -jnp.inf))
    scores = jnp.einsum("blgn,bsgn->blsg", queries_c, keys_b, precision=HIGHEST)
    inside = jnp.einsum("blsg,blsgr,bsgrp->blgrp", scores, decays, scaled_in, precision=HIGHEST)
    totals = running[:, -1]
    remain = jnp.exp(totals[:, None] - running)
    block_states = jnp.einsum(
        "bsgn,bsgr,bsgrp->bgrpn", keys_b, remain, scaled_in, precision=HIGHEST
    )

    def advance(carried, pieces):
        return (carried * jnp.exp(pieces[1])[..., None, None] + pieces[0], carried)

    initial = jnp.zeros(block_states.shape[1:], jnp.float32)
    own_state, entering = lax.scan(advance, initial, (block_states, totals))
    own_decay = jnp.exp(jnp.sum(totals, axis=0))
    _, incoming = prefix(
        (own_decay, own_state),
        "sp",
        link_states,
        (jnp.ones_like(own_decay), jnp.zeros_like(own_state)),
    )
    preceding = jnp.exp(jnp.cumsum(totals, axis=0) - totals)
    entering = entering + preceding[..., None, None] * incoming[None]
    outside = jnp.einsum(
        "blgn,bgrpn,blgr->blgrp", queries_c, entering, jnp.exp(running), precision=HIGHEST
    )
    return (inside + outside).reshape(length, -1)


def fetch_rows(tokens, sources):
    present = sources >= 0
    picked = jnp.take(tokens, jnp.maximum(sources, 0), axis=0)
    return jnp.where(present[:, None], picked, jnp.zeros_like(picked))


def slot_tables(chosen_ids, quarters, row_count, experts, capacity):
    picks = chosen_ids.shape[1]
    flat_ids = chosen_ids.reshape(quarters, row_count * picks)
    member = (flat_ids[..., None] == jnp.arange(experts, dtype=jnp.int32)).astype(jnp.int32)
    position = jnp.sum((jnp.cumsum(member, axis=1) - member) * member, axis=2)
    quarter_ids = jnp.arange(quarters, dtype=jnp.int32)[:, None]
    slot_index = flat_ids * (quarters * capacity) + quarter_ids * capacity + position
    token_index = (
        quarter_ids * row_count + jnp.arange(row_count * picks, dtype=jnp.int32)[None, :] // picks
    )
    sources = (
        jnp.full((experts * quarters * capacity,), -1, jnp.int32)
        .at[slot_index.reshape(-1)]
        .set(token_index.reshape(-1))
    )
    return (sources, position)


def per_device(
    carryover_vector,
    channel_source_entries,
    final_modulation_vector,
    entering_basis_matrix,
    readout_basis_matrix,
    raw_stride_amount,
    extra_log_attenuation,
    channel_fading_rate,
    channel_source_kernel,
    entering_basis_kernel,
    readout_basis_kernel,
    modulated_rescaling_vector,
    blender_final_matrix,
    specialist_rescaling_vector,
    specialist_gating_matrices,
    widening_matrices,
    contracting_matrices,
    assigned_specialist_ids,
    specialist_choice_affinity,
    cluster_chance,
):
    length = channel_source_entries.shape[0]
    row_count = carryover_vector.shape[0]
    model_width = carryover_vector.shape[1]
    heads_here = channel_fading_rate.shape[0]
    groups_here = entering_basis_matrix.shape[1] // STATE
    tp_index = lax.axis_index("tp")
    rim_rows = channel_source_kernel.shape[0] - 1
    neighbours = from_behind(
        (
            channel_source_entries[length - rim_rows :],
            entering_basis_matrix[length - rim_rows :],
            readout_basis_matrix[length - rim_rows :],
        ),
        "sp",
        1,
    )
    inputs_x = causal_conv(channel_source_entries, neighbours[0], channel_source_kernel)
    keys_b = causal_conv(entering_basis_matrix, neighbours[1], entering_basis_kernel)
    queries_c = causal_conv(readout_basis_matrix, neighbours[2], readout_basis_kernel)
    channel_stride_amount = jax.nn.softplus(raw_stride_amount)
    log_attenuation = extra_log_attenuation - channel_fading_rate[None, :] * channel_stride_amount
    heads_x = inputs_x.reshape(length, heads_here, HEAD_DIM)
    mixed = device_states(
        heads_x * channel_stride_amount[:, :, None], log_attenuation, keys_b, queries_c, groups_here
    )
    gated = mixed * jax.nn.silu(final_modulation_vector.astype(jnp.float32))
    head_cols = gated.shape[1]
    squares = lax.psum(jnp.sum(gated * gated, axis=1), "tp")
    first_col = tp_index * head_cols
    gain_part = lax.dynamic_slice_in_dim(modulated_rescaling_vector, first_col, head_cols, 0)
    scale = lax.rsqrt(squares / (head_cols * lax.axis_size("tp")) + EPS)
    normed = (gated * scale[:, None] * gain_part[None, :]).astype(jnp.bfloat16)
    weight_rows = lax.dynamic_slice_in_dim(blender_final_matrix, first_col, head_cols, 0)
    summed = lax.psum_scatter(
        jnp.dot(normed, weight_rows, preferred_element_type=jnp.float32).astype(jnp.bfloat16),
        "tp",
        scatter_dimension=0,
        tiled=True,
    ).astype(jnp.float32)
    middle = (carryover_vector.astype(jnp.float32) + summed).astype(jnp.bfloat16)
    middle_wide = middle.astype(jnp.float32)
    expert_input = (
        middle_wide
        * lax.rsqrt(jnp.mean(middle_wide * middle_wide, axis=1, keepdims=True) + EPS)
        * specialist_rescaling_vector[None, :]
    ).astype(jnp.bfloat16)
    sp_count = lax.axis_size("sp")
    local_experts = specialist_gating_matrices.shape[0]
    experts = sp_count * local_experts
    picks = assigned_specialist_ids.shape[1]
    capacity = 2 * row_count * picks // experts
    own_ids = lax.dynamic_slice_in_dim(assigned_specialist_ids, tp_index * row_count, row_count, 0)
    sources, position = slot_tables(own_ids, 1, row_count, experts, capacity)
    own_position = position[0]
    outgoing = fetch_rows(expert_input, sources).reshape(
        sp_count, local_experts, 1, capacity, model_width
    )
    received = lax.all_to_all(outgoing, "sp", split_axis=0, concat_axis=0, tiled=True)
    arrived = lax.all_gather(received, "tp", axis=2, tiled=True)
    gate_value = jnp.einsum(
        "slqcd,ldf->slqcf", arrived, specialist_gating_matrices, preferred_element_type=jnp.float32
    )
    up_value = jnp.einsum(
        "slqcd,ldf->slqcf", arrived, widening_matrices, preferred_element_type=jnp.float32
    )
    hidden = (jax.nn.silu(gate_value) * up_value).astype(jnp.bfloat16)
    partial_value = jnp.einsum(
        "slqcf,lfd->slqcd", hidden, contracting_matrices, preferred_element_type=jnp.float32
    )
    width_total = lax.psum_scatter(
        partial_value.astype(jnp.bfloat16), "tp", scatter_dimension=2, tiled=True
    )
    returned = lax.all_to_all(width_total, "sp", split_axis=0, concat_axis=0, tiled=True)
    answers = returned.reshape(experts * capacity, model_width)
    own_slots = own_ids.reshape(-1) * capacity + own_position
    gathered = (
        jnp.take(answers, own_slots, axis=0)
        .reshape(row_count, picks, model_width)
        .astype(jnp.float32)
    )
    lifted = jnp.exp(specialist_choice_affinity)
    shares = cluster_chance[:, None] * lifted / jnp.sum(lifted, axis=1, keepdims=True)
    return (middle_wide + jnp.sum(shares[:, :, None] * gathered, axis=1)).astype(jnp.bfloat16)


def solution(mesh):
    return jax.shard_map(
        per_device,
        mesh=mesh,
        in_specs=(
            P(("grp", "sp", "tp"), None),
            P(("grp", "sp"), "tp"),
            P(("grp", "sp"), "tp"),
            P(("grp", "sp"), "tp"),
            P(("grp", "sp"), "tp"),
            P(("grp", "sp"), "tp"),
            P(("grp", "sp"), "tp"),
            P("tp"),
            P(None, "tp"),
            P(None, "tp"),
            P(None, "tp"),
            P(),
            P(),
            P(),
            P("sp", None, "tp"),
            P("sp", None, "tp"),
            P("sp", "tp", None),
            P(("grp", "sp"), None),
            P(("grp", "sp", "tp"), None),
            P(("grp", "sp", "tp")),
        ),
        out_specs=P(("grp", "sp", "tp"), None),
        check_vma=False,
    )
```

profile of v0, /device:TPU:0, one launch (start us, length us, event | category | flops | bytes accessed | tf_op | source)
XLA Modules:
  0.0 319.8 jit_solution(16256433366509483427)
XLA Ops:
  7.4 4.9 %collective-permute-start.2 = (bf16[3,256]{1,0:T(4,128)(2,1)S(1)}, bf16[3,256]{1,0:T(4,128)(2,1)S(1)}, u32[]{:S(2)}, u32[]{:S(2)}) collective-permute-start(bf16[3,256]{1,0:T(4,128)(2,1)S(1)} %slice.103), channel_id=1, source_target_pairs={{0,4},{4,8},{8,12},{1,5},{5,9},{9,13},{2,6},{6,10},{10,14},{3,7},{... | collective-permute-start | bytes 4616 | tf_op jit(solution)/shard_map/ppermute | solution.py:35
  13.0 3.5 %collective-permute-start = (bf16[3,128]{1,0:T(4,128)(2,1)S(1)}, bf16[3,128]{1,0:T(4,128)(2,1)S(1)}, u32[]{:S(2)}, u32[]{:S(2)}) collective-permute-start(bf16[3,128]{1,0:T(4,128)(2,1)S(1)} %slice.85), channel_id=1, source_target_pairs={{0,4},{4,8},{8,12},{1,5},{5,9},{9,13},{2,6},{6,10},{10,14},{3,7},{... | collective-permute-start | bytes 2312 | tf_op jit(solution)/shard_map/ppermute | solution.py:35
  17.2 3.5 %collective-permute-start.1 = (bf16[3,128]{1,0:T(4,128)(2,1)S(1)}, bf16[3,128]{1,0:T(4,128)(2,1)S(1)}, u32[]{:S(2)}, u32[]{:S(2)}) collective-permute-start(bf16[3,128]{1,0:T(4,128)(2,1)S(1)} %slice.94), channel_id=1, source_target_pairs={{0,4},{4,8},{8,12},{1,5},{5,9},{9,13},{2,6},{6,10},{10,14},{3,7},{... | collective-permute-start | bytes 2312 | tf_op jit(solution)/shard_map/ppermute | solution.py:35
  27.7 8.4 %all-reduce = bf16[16]{0:T(256)(128)(2,1)S(1)} all-reduce(bf16[16]{0:T(256)(128)(2,1)S(1)} %dynamic-update-slice), channel_id=2, replica_groups=mesh['grp'=2,'sp'=4,'tp'=4] {'sp'}, use_global_device_ids=true, to_apply=%add | all-reduce | flops 16 | bytes 64
  44.8 1.5 convolution_bitcast_fusion
  46.4 5.6 %while.27 = (s32[]{:T(128)}, f32[1,4,64,128]{3,2,1,0:T(8,128)S(1)}, f32[4,1,4,64,128]{4,3,2,1,0:T(8,128)}, f32[4,1,4]{2,1,0:T(1,128)}, f32[4,1,4,64,128]{4,3,2,1,0:T(8,128)S(1)}, /*index=5*/s32[]{:T(128)}, s32[]{:T(128)}) while((s32[]{:T(128)}, f32[1,4,64,128]{3,2,1,0:T(8,128)S(1)}, f32[4,1,4,64,128]{4,3,2,1,0:T(8,128)}, ...), condition=%wide.region_2.3_spmd.clone, body=%wide.region_1.2_spmd.clone.sunk | while | flops 131075 | bytes 656016 | solution.py:76
  52.0 13.9 %all-gather.1 = bf16[4,4,64,128]{3,2,1,0:T(8,128)(2,1)S(1)} all-gather(bf16[1,4,64,128]{3,2,1,0:T(8,128)(2,1)S(1)} %convert_element_type.121), channel_id=3, replica_groups=mesh['grp'=2,'sp'=4,'tp'=4] {'sp'}, dimensions={0}, use_global_device_ids=true | all-gather | bytes 327680 | tf_op jit(solution)/shard_map/all_gather | solution.py:16
  66.0 3.0 while.28
  68.9 2.8 fusion.20
  71.7 2.0 fusion.21
  74.6 5.7 %psum.7 = f32[256]{0:T(256)S(1)} all-reduce(f32[256]{0:T(256)S(1)} %multiply_reduce_fusion.1), channel_id=1, replica_groups=mesh['grp'=2,'sp'=4,'tp'=4] {'tp'}, use_global_device_ids=true, to_apply=%region_8.9 | all-reduce | flops 256 | bytes 2048 | tf_op jit(solution)/shard_map/psum | solution.py:165
  80.3 2.7 convolution_convert_fusion
  85.3 22.6 %reduce-scatter.5.cloned.1.call-done = bf16[64,2048]{1,0:T(8,128)(2,1)} async-done(((bf16[256,2048]{1,0:T(8,128)(2,1)}), bf16[64,2048]{1,0:T(8,128)(2,1)}) %reduce-scatter.5.cloned.1.call-update) | async-done | bytes 262160 | tf_op jit(solution)/shard_map/reduce_scatter | solution.py:171
  111.8 30.0 %all_to_all.10 = bf16[4,2,1,32,2048]{4,3,2,1,0:T(8,128)(2,1)S(1)} all-to-all(bf16[4,2,1,32,2048]{4,3,2,1,0:T(8,128)(2,1)S(1)} %select_bitcast_fusion), channel_id=1, replica_groups=mesh['grp'=2,'sp'=4,'tp'=4] {'sp'}, dimensions={0} | all-to-all | bytes 2097152 | tf_op jit(solution)/shard_map/all_to_all | solution.py:195
  143.1 32.5 %all-gather.4.cloned.1.call-done = bf16[4,2,4,32,2048]{4,3,2,0,1:T(8,128)(2,1)} async-done(((bf16[4,2,1,32,2048]{4,3,2,0,1:T(8,128)(2,1)}), bf16[4,2,4,32,2048]{4,3,2,0,1:T(8,128)(2,1)}) %all-gather.4.cloned.1.call-update) | async-done | bytes 4194320 | tf_op jit(solution)/shard_map/all_gather | solution.py:196
  175.6 4.1 %fusion.8 = f32[4,2,4,32,256]{4,3,2,0,1:T(8,128)S(1)} fusion(bf16[4,2,4,32,2048]{4,3,2,0,1:T(8,128)(2,1)} %all-gather.4.cloned.1.call-done, bf16[2,2048,256]{2,1,0:T(8,128)(2,1)} %param.38), kind=kOutput, calls=%fused_computation.18 | convolution fusion | flops 1073741824 | bytes 7340032 | tf_op jit(solution)/shard_map/slqcd,ldf->slqcf/dot_general | solution.py:197
  179.7 7.3 %convert_bitcast_fusion = bf16[4,2,4,32,2048]{4,3,2,0,1:T(8,128)(2,1)} fusion(bf16[2,256,2048]{2,1,0:T(8,128)(2,1)S(1)} %copy-done, bf16[4,2,4,32,2048]{4,3,2,0,1:T(8,128)(2,1)} %all-gather.4.cloned.1.call-done, bf16[2,2048,256]{2,1,0:T(8,128)(2,1)} %param.39, f32[4,2,4,32,256]{4,3,2,0,1:T(8,128)S(1)} %fusion.8), kind=kOutput, calls=%fused_computation.11 | convolution fusion | flops 2151153664 | bytes 13631488 | tf_op jit(solution)/shard_map/slqcf,lfd->slqcd/dot_general | solution.py:204
  188.3 84.4 %all-reduce.4.cloned.1.call-done = bf16[4,2,4,32,2048]{4,3,2,0,1:T(8,128)(2,1)} async-done(((bf16[4,2,4,32,2048]{4,3,2,0,1:T(8,128)(2,1)}), bf16[4,2,4,32,2048]{4,3,2,0,1:T(8,128)(2,1)}) %all-reduce.4.cloned.1.call-update) | async-done | bytes 4194320
  272.7 1.9 constant_dynamic-slice_fusion.1
  275.7 4.7 %all-to-all-start.1 = ((bf16[4,2,1,32,2048]{4,3,2,1,0:T(8,128)(2,1)}), bf16[4,2,1,32,2048]{4,3,2,1,0:T(8,128)(2,1)S(1)}, u32[]{:S(2)}, u32[]{:S(2)}) async-start(bf16[4,2,1,32,2048]{4,3,2,1,0:T(8,128)(2,1)} %copy.94), calls=%async_computation.2 | async-start | bytes 2097152 | tf_op jit(solution)/shard_map/all_to_all | solution.py:210
  280.9 24.9 %all-to-all-done.1 = bf16[4,2,1,32,2048]{4,3,2,1,0:T(8,128)(2,1)S(1)} async-done(((bf16[4,2,1,32,2048]{4,3,2,1,0:T(8,128)(2,1)}), bf16[4,2,1,32,2048]{4,3,2,1,0:T(8,128)(2,1)S(1)}, u32[]{:S(2)}, u32[]{:S(2)}) %all-to-all-start.1) | async-done | bytes 1048608 | tf_op jit(solution)/shard_map/all_to_all | solution.py:210
  305.8 1.7 gather_fusion.1
  308.9 2.5 multiply_reduce_fusion
  311.5 1.8 fusion.28
  (127 shorter events, 37.9 us)
Async XLA Ops:
  6.5 173.2 %copy-start = (bf16[2,256,2048]{2,1,0:T(8,128)(2,1)S(1)}, bf16[2,256,2048]{2,1,0:T(8,128)(2,1)}, u32[]{:S(2)}) copy-start(bf16[2,256,2048]{2,1,0:T(8,128)(2,1)} %param.40) | copy-start | bytes 6291460
  6.5 101.4 %reduce-scatter.5.cloned.1.call-start = ((), (), s32[]{:S(2)}) async-start(), calls=%async_computation.3 | async-start | bytes 1310720 | tf_op jit(solution)/shard_map/reduce_scatter | solution.py:171
  7.4 35.9 %collective-permute-start.2 = (bf16[3,256]{1,0:T(4,128)(2,1)S(1)}, bf16[3,256]{1,0:T(4,128)(2,1)S(1)}, u32[]{:S(2)}, u32[]{:S(2)}) collective-permute-start(bf16[3,256]{1,0:T(4,128)(2,1)S(1)} %slice.103), channel_id=1, source_target_pairs={{0,4},{4,8},{8,12},{1,5},{5,9},{9,13},{2,6},{6,10},{10,14},{3,7},{... | collective-permute-start | bytes 4616 | tf_op jit(solution)/shard_map/ppermute | solution.py:35
  13.0 27.1 %collective-permute-start = (bf16[3,128]{1,0:T(4,128)(2,1)S(1)}, bf16[3,128]{1,0:T(4,128)(2,1)S(1)}, u32[]{:S(2)}, u32[]{:S(2)}) collective-permute-start(bf16[3,128]{1,0:T(4,128)(2,1)S(1)} %slice.85), channel_id=1, source_target_pairs={{0,4},{4,8},{8,12},{1,5},{5,9},{9,13},{2,6},{6,10},{10,14},{3,7},{... | collective-permute-start | bytes 2312 | tf_op jit(solution)/shard_map/ppermute | solution.py:35
  17.2 24.0 %collective-permute-start.1 = (bf16[3,128]{1,0:T(4,128)(2,1)S(1)}, bf16[3,128]{1,0:T(4,128)(2,1)S(1)}, u32[]{:S(2)}, u32[]{:S(2)}) collective-permute-start(bf16[3,128]{1,0:T(4,128)(2,1)S(1)} %slice.94), channel_id=1, source_target_pairs={{0,4},{4,8},{8,12},{1,5},{5,9},{9,13},{2,6},{6,10},{10,14},{3,7},{... | collective-permute-start | bytes 2312 | tf_op jit(solution)/shard_map/ppermute | solution.py:35
  41.1 1.0 copy-start.3
  52.0 22.5 %copy-start.4 = (bf16[256,256]{1,0:T(8,128)(2,1)S(1)}, bf16[256,256]{1,0:T(8,128)(2,1)}, u32[]{:S(2)}) copy-start(bf16[256,256]{1,0:T(8,128)(2,1)} %param.26) | copy-start | bytes 393220
  52.0 28.3 %copy-start.7 = (f32[256]{0:T(256)S(1)}, f32[256]{0:T(256)}, u32[]{:S(2)}) copy-start(f32[256]{0:T(256)} %dynamic_slice.31) | copy-start | bytes 3076
  68.9 14.2 %copy-start.8 = (s32[256,2]{0,1:T(2,128)S(1)}, s32[256,2]{0,1:T(2,128)}, u32[]{:S(2)}) copy-start(s32[256,2]{0,1:T(2,128)} %param.41) | copy-start | bytes 6148
  71.7 36.3 %copy-start.1 = (bf16[64,2048]{1,0:T(8,128)(2,1)S(1)}, bf16[64,2048]{1,0:T(8,128)(2,1)}, u32[]{:S(2)}) copy-start(bf16[64,2048]{1,0:T(8,128)(2,1)} %param.24) | copy-start | bytes 786436
  71.7 37.4 %copy-start.5 = (f32[2048]{0:T(1024)S(1)}, f32[2048]{0:T(1024)}, u32[]{:S(2)}) copy-start(f32[2048]{0:T(1024)} %param.37) | copy-start | bytes 24580
  83.1 92.5 %all-gather.4.cloned.1.call-start = ((), (), s32[]{:S(2)}) async-start(), calls=%async_computation.4 | async-start | bytes 5242880 | tf_op jit(solution)/shard_map/all_gather | solution.py:196
  142.8 129.8 %all-reduce.4.cloned.1.call-start = ((), (), s32[]{:S(2)}) async-start(), calls=%async_computation.5 | async-start | bytes 8388608
  187.0 0.7 copy-start.10
  187.0 93.7 %copy-start.6 = (f32[64,2]{0,1:T(2,128)S(1)}, f32[64,2]{0,1:T(2,128)}, u32[]{:S(2)}) copy-start(f32[64,2]{0,1:T(2,128)} %param.42) | copy-start | bytes 1540
  187.1 93.7 %copy-start.9 = (f32[64]{0:T(128)S(1)}, f32[64]{0:T(128)}, u32[]{:S(2)}) copy-start(f32[64]{0:T(128)} %param.43) | copy-start | bytes 772
  275.7 35.8 %copy-start.2 = (bf16[64,2048]{1,0:T(8,128)(2,1)S(1)}, bf16[64,2048]{1,0:T(8,128)(2,1)}, u32[]{:S(2)}) copy-start(bf16[64,2048]{1,0:T(8,128)(2,1)} %param.24) | copy-start | bytes 786436
  275.7 30.1 %all-to-all-start.1 = ((bf16[4,2,1,32,2048]{4,3,2,1,0:T(8,128)(2,1)}), bf16[4,2,1,32,2048]{4,3,2,1,0:T(8,128)(2,1)S(1)}, u32[]{:S(2)}, u32[]{:S(2)}) async-start(bf16[4,2,1,32,2048]{4,3,2,1,0:T(8,128)(2,1)} %copy.94), calls=%async_computation.2 | async-start | bytes 2097152 | tf_op jit(solution)/shard_map/all_to_all | solution.py:210
Sparse Core Ops, SparseCore 0:
  83.2 24.7 reduce-scatter.4
  143.0 32.5 all-gather.3
  187.2 85.4 all-reduce.3
where the time goes:
time: 321 us; the launch traced here: 320 us
  waiting for transfers between devices  165 us (51%)
  blocking collectives  57.9 us (18%)
  local copies, waits for them, and re-layouts  26.1 us (8%)
  matrix products  20.8 us (6%)
  other arithmetic  19.1 us (6%)
  starting transfers between devices  16.9 us (5%)
  between operations  14.2 us (4%)
    unnamed x4, waiting for transfers between devices  84.5 us
    all_gather x1, waiting for transfers between devices, per_device(): arrived = lax.all_gather(received, 'tp', axis=2, tiled=True)  32.5 us
    all_to_all x1, blocking collectives, per_device(): lax.all_to_all(outgoing, 'sp', split_axis=0, concat_axis=0, tiled=True)  30 us
    all_to_all x1, waiting for transfers between devices, per_device(): lax.all_to_all(width_total, 'sp', split_axis=0, concat_axis=0, tiled=True)  24.9 us
    reduce_scatter x1, waiting for transfers between devices, per_device(): lax.psum_scatter(jnp.dot(normed, weight_rows, preferred_element_type=jnp....  22.6 us
    all_gather x1, blocking collectives, prefix(): lax.all_gather(part.astype(kind), axis)  13.9 us
    ppermute x3, starting transfers between devices, from_behind(): return lax.ppermute(x, axis, pairs)  11.9 us
    unnamed x1, blocking collectives  8.36 us
  transfers between devices with their start and end apart: 7, of which 4 were waited for; matrix products, arithmetic and copies ran while one was open for 6% of the time, Pallas kernels for 0%

commit v1 on v0

--- a/solution.py
+++ b/solution.py
@@ -193,7 +193,7 @@
         sp_count, local_experts, 1, capacity, model_width
     )
     received = lax.all_to_all(outgoing, "sp", split_axis=0, concat_axis=0, tiled=True)
-    arrived = lax.all_gather(received, "tp", axis=2, tiled=True)
+    arrived = jnp.concatenate(lax.all_gather(received, "tp"), axis=2)
     gate_value = jnp.einsum(
         "slqcd,ldf->slqcf", arrived, specialist_gating_matrices, preferred_element_type=jnp.float32
     )

time: 321 us -> 320 us (level)
  no operation moved by 1% of the time
where the time goes in v1:
time: 320 us; the launch traced here: 319 us
  waiting for transfers between devices  165 us (52%)
  blocking collectives  58 us (18%)
  local copies, waits for them, and re-layouts  25 us (8%)
  matrix products  20.8 us (6%)
  other arithmetic  19.1 us (6%)
  starting transfers between devices  16.9 us (5%)
  between operations  14.2 us (4%)
    unnamed x4, waiting for transfers between devices  84.5 us
    all_gather x1, waiting for transfers between devices, per_device(): arrived = jnp.concatenate(lax.all_gather(received, 'tp'), axis=2)  32.5 us
    all_to_all x1, blocking collectives, per_device(): lax.all_to_all(outgoing, 'sp', split_axis=0, concat_axis=0, tiled=True)  30.1 us
    all_to_all x1, waiting for transfers between devices, per_device(): lax.all_to_all(width_total, 'sp', split_axis=0, concat_axis=0, tiled=True)  24.9 us
    reduce_scatter x1, waiting for transfers between devices, per_device(): lax.psum_scatter(jnp.dot(normed, weight_rows, preferred_element_type=jnp....  22.6 us
    all_gather x1, blocking collectives, prefix(): lax.all_gather(part.astype(kind), axis)  13.9 us
    ppermute x3, starting transfers between devices, from_behind(): return lax.ppermute(x, axis, pairs)  11.9 us
    unnamed x1, blocking collectives  8.36 us
  transfers between devices with their start and end apart: 7, of which 4 were waited for; matrix products, arithmetic and copies ran while one was open for 6% of the time, Pallas kernels for 0%

profile of v1, /device:TPU:0, one launch (start us, length us, event | category | flops | bytes accessed | tf_op | source)
XLA Modules:
  0.0 318.8 jit_solution(6473657620886182021)
XLA Ops:
  7.4 4.9 %collective-permute-start.2 = (bf16[3,256]{1,0:T(4,128)(2,1)S(1)}, bf16[3,256]{1,0:T(4,128)(2,1)S(1)}, u32[]{:S(2)}, u32[]{:S(2)}) collective-permute-start(bf16[3,256]{1,0:T(4,128)(2,1)S(1)} %slice.103), channel_id=1, source_target_pairs={{0,4},{4,8},{8,12},{1,5},{5,9},{9,13},{2,6},{6,10},{10,14},{3,7},{... | collective-permute-start | bytes 4616 | tf_op jit(solution)/shard_map/ppermute | solution.py:35
  13.0 3.5 %collective-permute-start = (bf16[3,128]{1,0:T(4,128)(2,1)S(1)}, bf16[3,128]{1,0:T(4,128)(2,1)S(1)}, u32[]{:S(2)}, u32[]{:S(2)}) collective-permute-start(bf16[3,128]{1,0:T(4,128)(2,1)S(1)} %slice.85), channel_id=1, source_target_pairs={{0,4},{4,8},{8,12},{1,5},{5,9},{9,13},{2,6},{6,10},{10,14},{3,7},{... | collective-permute-start | bytes 2312 | tf_op jit(solution)/shard_map/ppermute | solution.py:35
  17.2 3.5 %collective-permute-start.1 = (bf16[3,128]{1,0:T(4,128)(2,1)S(1)}, bf16[3,128]{1,0:T(4,128)(2,1)S(1)}, u32[]{:S(2)}, u32[]{:S(2)}) collective-permute-start(bf16[3,128]{1,0:T(4,128)(2,1)S(1)} %slice.94), channel_id=1, source_target_pairs={{0,4},{4,8},{8,12},{1,5},{5,9},{9,13},{2,6},{6,10},{10,14},{3,7},{... | collective-permute-start | bytes 2312 | tf_op jit(solution)/shard_map/ppermute | solution.py:35
  27.7 8.4 %all-reduce = bf16[16]{0:T(256)(128)(2,1)S(1)} all-reduce(bf16[16]{0:T(256)(128)(2,1)S(1)} %dynamic-update-slice), channel_id=2, replica_groups=mesh['grp'=2,'sp'=4,'tp'=4] {'sp'}, use_global_device_ids=true, to_apply=%add | all-reduce | flops 16 | bytes 64
  44.8 1.5 convolution_bitcast_fusion
  46.4 5.6 %while.27 = (s32[]{:T(128)}, f32[1,4,64,128]{3,2,1,0:T(8,128)S(1)}, f32[4,1,4,64,128]{4,3,2,1,0:T(8,128)}, f32[4,1,4]{2,1,0:T(1,128)}, f32[4,1,4,64,128]{4,3,2,1,0:T(8,128)S(1)}, /*index=5*/s32[]{:T(128)}, s32[]{:T(128)}) while((s32[]{:T(128)}, f32[1,4,64,128]{3,2,1,0:T(8,128)S(1)}, f32[4,1,4,64,128]{4,3,2,1,0:T(8,128)}, ...), condition=%wide.region_2.3_spmd.clone, body=%wide.region_1.2_spmd.clone.sunk | while | flops 131075 | bytes 656016 | solution.py:76
  52.0 13.9 %all-gather.1 = bf16[4,4,64,128]{3,2,1,0:T(8,128)(2,1)S(1)} all-gather(bf16[1,4,64,128]{3,2,1,0:T(8,128)(2,1)S(1)} %convert_element_type.121), channel_id=3, replica_groups=mesh['grp'=2,'sp'=4,'tp'=4] {'sp'}, dimensions={0}, use_global_device_ids=true | all-gather | bytes 327680 | tf_op jit(solution)/shard_map/all_gather | solution.py:16
  66.0 3.0 while.28
  68.9 2.8 fusion.32
  71.7 2.0 fusion.33
  74.6 5.7 %psum.7 = f32[256]{0:T(256)S(1)} all-reduce(f32[256]{0:T(256)S(1)} %multiply_reduce_fusion.1), channel_id=1, replica_groups=mesh['grp'=2,'sp'=4,'tp'=4] {'tp'}, use_global_device_ids=true, to_apply=%region_8.9 | all-reduce | flops 256 | bytes 2048 | tf_op jit(solution)/shard_map/psum | solution.py:165
  80.3 2.7 convolution_convert_fusion
  85.3 22.6 %reduce-scatter.5.cloned.1.call-done = bf16[64,2048]{1,0:T(8,128)(2,1)} async-done(((bf16[256,2048]{1,0:T(8,128)(2,1)}), bf16[64,2048]{1,0:T(8,128)(2,1)}) %reduce-scatter.5.cloned.1.call-update) | async-done | bytes 262160 | tf_op jit(solution)/shard_map/reduce_scatter | solution.py:171
  111.8 30.1 %all_to_all.10 = bf16[4,2,1,32,2048]{4,3,1,2,0:T(8,128)(2,1)} all-to-all(bf16[4,2,1,32,2048]{4,3,1,2,0:T(8,128)(2,1)S(1)} %select_select_fusion), channel_id=1, replica_groups=mesh['grp'=2,'sp'=4,'tp'=4] {'sp'}, dimensions={0} | all-to-all | bytes 2097152 | tf_op jit(solution)/shard_map/all_to_all | solution.py:195
  142.1 32.5 %all-gather.5.cloned.1.call-done = bf16[16,2,1,32,2048]{4,3,2,1,0:T(8,128)(2,1)} async-done(((bf16[4,2,1,32,2048]{4,3,2,1,0:T(8,128)(2,1)}), bf16[16,2,1,32,2048]{4,3,2,1,0:T(8,128)(2,1)}) %all-gather.5.cloned.1.call-update) | async-done | bytes 4194320 | tf_op jit(solution)/shard_map/all_gather | solution.py:196
  174.6 4.1 %fusion.12 = f32[4,2,4,32,256]{4,3,2,0,1:T(8,128)S(1)} fusion(bf16[2,2048,256]{2,1,0:T(8,128)(2,1)} %param.38, bf16[4,4,2,1,32,2048]{5,4,2,1,0,3:T(8,128)(2,1)} %bitcast.188), kind=kOutput, calls=%fused_computation.22 | convolution fusion | flops 1073741824 | bytes 7340032 | tf_op jit(solution)/shard_map/slqcd,ldf->slqcf/dot_general | solution.py:197
  178.8 7.3 %convert_bitcast_fusion = bf16[4,2,4,32,2048]{4,3,2,0,1:T(8,128)(2,1)} fusion(bf16[2,256,2048]{2,1,0:T(8,128)(2,1)S(1)} %copy-done, bf16[2,2048,256]{2,1,0:T(8,128)(2,1)} %param.39, bf16[4,4,2,1,32,2048]{5,4,2,1,0,3:T(8,128)(2,1)} %bitcast.189, f32[4,2,4,32,256]{4,3,2,0,1:T(8,128)S(1)} %fusion.12), kind=kOutput, calls=%fused_computation.15 | convolution fusion | flops 2151153664 | bytes 13631488 | tf_op jit(solution)/shard_map/slqcf,lfd->slqcd/dot_general | solution.py:204
  187.3 84.4 %all-reduce.4.cloned.1.call-done = bf16[4,2,4,32,2048]{4,3,2,0,1:T(8,128)(2,1)} async-done(((bf16[4,2,4,32,2048]{4,3,2,0,1:T(8,128)(2,1)}), bf16[4,2,4,32,2048]{4,3,2,0,1:T(8,128)(2,1)}) %all-reduce.4.cloned.1.call-update) | async-done | bytes 4194320
  271.7 1.9 constant_dynamic-slice_fusion.1
  274.7 4.7 %all-to-all-start.1 = ((bf16[4,2,1,32,2048]{4,3,2,1,0:T(8,128)(2,1)}), bf16[4,2,1,32,2048]{4,3,2,1,0:T(8,128)(2,1)S(1)}, u32[]{:S(2)}, u32[]{:S(2)}) async-start(bf16[4,2,1,32,2048]{4,3,2,1,0:T(8,128)(2,1)} %copy.94), calls=%async_computation.2 | async-start | bytes 2097152 | tf_op jit(solution)/shard_map/all_to_all | solution.py:210
  280.0 24.9 %all-to-all-done.1 = bf16[4,2,1,32,2048]{4,3,2,1,0:T(8,128)(2,1)S(1)} async-done(((bf16[4,2,1,32,2048]{4,3,2,1,0:T(8,128)(2,1)}), bf16[4,2,1,32,2048]{4,3,2,1,0:T(8,128)(2,1)S(1)}, u32[]{:S(2)}, u32[]{:S(2)}) %all-to-all-start.1) | async-done | bytes 1048608 | tf_op jit(solution)/shard_map/all_to_all | solution.py:210
  304.9 1.7 gather_fusion.1
  308.0 2.5 multiply_reduce_fusion
  310.5 1.8 fusion.45
  (126 shorter events, 36.9 us)
Async XLA Ops:
  6.5 172.2 %copy-start = (bf16[2,256,2048]{2,1,0:T(8,128)(2,1)S(1)}, bf16[2,256,2048]{2,1,0:T(8,128)(2,1)}, u32[]{:S(2)}) copy-start(bf16[2,256,2048]{2,1,0:T(8,128)(2,1)} %param.40) | copy-start | bytes 6291460
  6.5 101.4 %reduce-scatter.5.cloned.1.call-start = ((), (), s32[]{:S(2)}) async-start(), calls=%async_computation.3 | async-start | bytes 1310720 | tf_op jit(solution)/shard_map/reduce_scatter | solution.py:171
  7.4 35.9 %collective-permute-start.2 = (bf16[3,256]{1,0:T(4,128)(2,1)S(1)}, bf16[3,256]{1,0:T(4,128)(2,1)S(1)}, u32[]{:S(2)}, u32[]{:S(2)}) collective-permute-start(bf16[3,256]{1,0:T(4,128)(2,1)S(1)} %slice.103), channel_id=1, source_target_pairs={{0,4},{4,8},{8,12},{1,5},{5,9},{9,13},{2,6},{6,10},{10,14},{3,7},{... | collective-permute-start | bytes 4616 | tf_op jit(solution)/shard_map/ppermute | solution.py:35
  13.0 27.1 %collective-permute-start = (bf16[3,128]{1,0:T(4,128)(2,1)S(1)}, bf16[3,128]{1,0:T(4,128)(2,1)S(1)}, u32[]{:S(2)}, u32[]{:S(2)}) collective-permute-start(bf16[3,128]{1,0:T(4,128)(2,1)S(1)} %slice.85), channel_id=1, source_target_pairs={{0,4},{4,8},{8,12},{1,5},{5,9},{9,13},{2,6},{6,10},{10,14},{3,7},{... | collective-permute-start | bytes 2312 | tf_op jit(solution)/shard_map/ppermute | solution.py:35
  17.2 24.0 %collective-permute-start.1 = (bf16[3,128]{1,0:T(4,128)(2,1)S(1)}, bf16[3,128]{1,0:T(4,128)(2,1)S(1)}, u32[]{:S(2)}, u32[]{:S(2)}) collective-permute-start(bf16[3,128]{1,0:T(4,128)(2,1)S(1)} %slice.94), channel_id=1, source_target_pairs={{0,4},{4,8},{8,12},{1,5},{5,9},{9,13},{2,6},{6,10},{10,14},{3,7},{... | collective-permute-start | bytes 2312 | tf_op jit(solution)/shard_map/ppermute | solution.py:35
  41.1 1.0 copy-start.3
  52.0 22.5 %copy-start.4 = (bf16[256,256]{1,0:T(8,128)(2,1)S(1)}, bf16[256,256]{1,0:T(8,128)(2,1)}, u32[]{:S(2)}) copy-start(bf16[256,256]{1,0:T(8,128)(2,1)} %param.26) | copy-start | bytes 393220
  52.0 28.3 %copy-start.7 = (f32[256]{0:T(256)S(1)}, f32[256]{0:T(256)}, u32[]{:S(2)}) copy-start(f32[256]{0:T(256)} %dynamic_slice.31) | copy-start | bytes 3076
  68.9 14.2 %copy-start.8 = (s32[256,2]{0,1:T(2,128)S(1)}, s32[256,2]{0,1:T(2,128)}, u32[]{:S(2)}) copy-start(s32[256,2]{0,1:T(2,128)} %param.41) | copy-start | bytes 6148
  71.7 36.3 %copy-start.1 = (bf16[64,2048]{1,0:T(8,128)(2,1)S(1)}, bf16[64,2048]{1,0:T(8,128)(2,1)}, u32[]{:S(2)}) copy-start(bf16[64,2048]{1,0:T(8,128)(2,1)} %param.24) | copy-start | bytes 786436
  71.7 37.4 %copy-start.5 = (f32[2048]{0:T(1024)S(1)}, f32[2048]{0:T(1024)}, u32[]{:S(2)}) copy-start(f32[2048]{0:T(1024)} %param.37) | copy-start | bytes 24580
  83.1 91.6 %all-gather.5.cloned.1.call-start = ((), (), s32[]{:S(2)}) async-start(), calls=%async_computation.4 | async-start | bytes 5242880 | tf_op jit(solution)/shard_map/all_gather | solution.py:196
  141.9 129.8 %all-reduce.4.cloned.1.call-start = ((), (), s32[]{:S(2)}) async-start(), calls=%async_computation.5 | async-start | bytes 8388608
  186.1 0.7 copy-start.10
  186.1 93.7 %copy-start.6 = (f32[64,2]{0,1:T(2,128)S(1)}, f32[64,2]{0,1:T(2,128)}, u32[]{:S(2)}) copy-start(f32[64,2]{0,1:T(2,128)} %param.42) | copy-start | bytes 1540
  186.1 93.7 %copy-start.9 = (f32[64]{0:T(128)S(1)}, f32[64]{0:T(128)}, u32[]{:S(2)}) copy-start(f32[64]{0:T(128)} %param.43) | copy-start | bytes 772
  274.7 35.8 %copy-start.2 = (bf16[64,2048]{1,0:T(8,128)(2,1)S(1)}, bf16[64,2048]{1,0:T(8,128)(2,1)}, u32[]{:S(2)}) copy-start(bf16[64,2048]{1,0:T(8,128)(2,1)} %param.24) | copy-start | bytes 786436
  274.7 30.1 %all-to-all-start.1 = ((bf16[4,2,1,32,2048]{4,3,2,1,0:T(8,128)(2,1)}), bf16[4,2,1,32,2048]{4,3,2,1,0:T(8,128)(2,1)S(1)}, u32[]{:S(2)}, u32[]{:S(2)}) async-start(bf16[4,2,1,32,2048]{4,3,2,1,0:T(8,128)(2,1)} %copy.94), calls=%async_computation.2 | async-start | bytes 2097152 | tf_op jit(solution)/shard_map/all_to_all | solution.py:210
Sparse Core Ops, SparseCore 0:
  83.2 24.7 reduce-scatter.4
  142.0 32.5 all-gather.4
  186.2 85.4 all-reduce.3
